TPU v7x, 1024 devices: a whole 4x4x32 slice. The times are simulated.
1024 devices in a mesh: ep: 64 (over z, core), tp: 16 (over y, x).
Axes of the slice: x: 4, y: 4, z: 32, core: 2. Of those that a mesh axis runs over, the one named last changes fastest.
Arguments:
- tokens: bfloat16 [768, 4096], P('ep', 'tp')
- norm_gain: float32 [4096], P('tp'), may hold values from 0.1 to 1.9
- routes: int32 [768, 6], P('ep'), may hold values from 0 to 63, all different within a row; in each aligned block of 12 rows (0 to 11, 12 to 23, ...) at most 2 rows name the same one
- route_weights: float32 [768, 6], P('ep'), may hold values from 0.05 to 1
- expert_gate: bfloat16 [64, 4096, 1024], P('ep', 'tp'), may hold values from -0.09375 to 0.09375
- expert_up: bfloat16 [64, 4096, 1024], P('ep', 'tp'), may hold values from -0.09375 to 0.09375
- expert_down: bfloat16 [64, 1024, 4096], P('ep', None, 'tp'), may hold values from -0.1875 to 0.1875
- shared_gate: bfloat16 [4096, 1024], P('tp'), may hold values from -0.09375 to 0.09375
- shared_up: bfloat16 [4096, 1024], P('tp'), may hold values from -0.09375 to 0.09375
- shared_down: bfloat16 [1024, 4096], P(None, 'tp'), may hold values from -0.1875 to 0.1875
Outputs:
- mixed: bfloat16 [768, 4096], P('ep', 'tp')
Inputs may be any that keep to these rules, and one draw needn't show every extreme that they name: `routes`: each row names 6 different experts; among the rows of one device no expert is named more than 2 times, and in some devices' rows one expert is named exactly 2 times.
All inputs are finite; a program needn't handle non-finite values.
Results may differ from a plain program's by a relative error of at most 0.0068.
Values may be sent and summed in bfloat16 or wider, within the bound.
A program may use at most 32 MiB of HBM per device.

v0:
```python
import functools

import jax
import jax.numpy as jnp
from jax import lax
from jax.sharding import Mesh
from jax.sharding import PartitionSpec as P

TP = ("tp_0", "tp_1")


def cut_along(x, dim, count):
    before, after = (x.shape[:dim], x.shape[dim + 1 :])
    return jnp.moveaxis(x.reshape(*before, count, -1, *after), dim, 0)


def summed_on_arrival(x, axis, dim):
    tiles = cut_along(x, dim, lax.axis_size(axis))
    arrived = lax.all_to_all(tiles, axis, split_axis=0, concat_axis=0, tiled=True)
    return arrived.sum(axis=0)


def side_by_side(arrays, axis, dim, along):
    ends, at = ([], 0)
    for a in arrays[:-1]:
        at += a.shape[along]
        ends.append(at)
    both = jnp.concatenate(arrays, axis=along)
    return tuple(jnp.split(summed_on_arrival(both, axis, dim), ends, axis=along))


def joined_along(tiles, dim):
    lengths = list(tiles.shape[1:])
    lengths[dim] *= tiles.shape[0]
    return jnp.moveaxis(tiles, 0, dim).reshape(lengths)


def sent_to_all(x, axis):
    copies = jnp.broadcast_to(x, (lax.axis_size(axis), *x.shape))
    return lax.all_to_all(copies, axis, split_axis=0, concat_axis=0, tiled=True)


def collect(x, axis, dim):
    return joined_along(sent_to_all(x, axis), dim)


def one_axis_at_a_time(x, axes):
    return functools.reduce(lax.psum, axes, x)


def of_everyone(x, axis):
    return sent_to_all(x, axis).sum(axis=0)


def in_one(arrays, axis):
    flat, at, gathered = (jnp.concatenate([a.reshape(-1) for a in arrays]), 0, [])
    running = of_everyone(flat, axis)
    for a in arrays:
        gathered.append(running[at : at + a.size].reshape(a.shape))
        at += a.size
    return tuple(gathered)


def block_ranks(route_blocks, n_experts):
    onehot = (route_blocks[..., None] == jnp.arange(n_experts, dtype=jnp.int32)).astype(jnp.int32)
    before = jnp.cumsum(onehot, axis=1) - onehot
    return jnp.sum(before * onehot, axis=-1)


def expert_rows(rows, gate_w, up_w, down_w):
    part_gate = jnp.dot(rows, gate_w, preferred_element_type=jnp.float32)
    part_up = jnp.dot(rows, up_w, preferred_element_type=jnp.float32)
    gate, up = side_by_side((part_gate, part_up), TP, 1, 0)
    hidden_part = (jax.nn.silu(gate) * up).astype(jnp.bfloat16)
    result = jnp.dot(collect(hidden_part, TP, 1), down_w, preferred_element_type=jnp.float32)
    return result.astype(jnp.bfloat16)


def local(
    tokens,
    norm_gain,
    routes,
    route_weights,
    expert_gate,
    expert_up,
    expert_down,
    shared_gate,
    shared_up,
    shared_down,
):
    tok_rows, part_width = tokens.shape
    picks = routes.shape[1]
    width = part_width * lax.axis_size(TP)
    n_experts = lax.axis_size("ep")
    capacity = max(2, tok_rows * picks // n_experts + 1)
    values = tokens.astype(jnp.float32)
    total = one_axis_at_a_time(jnp.sum(values * values, axis=1), TP)
    normed = (values * lax.rsqrt(total / width + 1e-06)[:, None] * norm_gain[None, :]).astype(
        jnp.bfloat16
    )
    scaled = 2.5 * route_weights / jnp.sum(route_weights, axis=1, keepdims=True)
    part_gate = jnp.dot(normed, shared_gate, preferred_element_type=jnp.float32)
    part_up = jnp.dot(normed, shared_up, preferred_element_type=jnp.float32)
    shared_g, shared_u = in_one((part_gate, part_up), TP)
    shared_hidden = (jax.nn.silu(shared_g) * shared_u).astype(jnp.bfloat16)
    shared_out = jnp.dot(shared_hidden, shared_down, preferred_element_type=jnp.float32)
    gate_w, up_w, down_w = (expert_gate[0], expert_up[0], expert_down[0])
    ranks = block_ranks(routes.reshape(1, tok_rows * picks), n_experts).reshape(tok_rows, picks)
    target = routes * capacity + ranks
    slots = jnp.arange(n_experts * capacity, dtype=jnp.int32)
    hits = target[:, :, None] == slots[None, None, :]
    select = jnp.any(hits, axis=1).astype(jnp.bfloat16)
    combine = jnp.sum(jnp.where(hits, scaled[:, :, None], 0.0), axis=1)
    outgoing = jnp.einsum("tj,td->jd", select, normed, preferred_element_type=jnp.float32)
    outgoing = outgoing.astype(jnp.bfloat16).reshape(n_experts, capacity, part_width)
    arrived = lax.all_to_all(outgoing, "ep", split_axis=0, concat_axis=0, tiled=True)
    rows = arrived.reshape(-1, part_width)
    result = expert_rows(rows, gate_w, up_w, down_w).reshape(arrived.shape)
    back = lax.all_to_all(result, "ep", split_axis=0, concat_axis=0, tiled=True)
    back_rows = back.reshape(n_experts * capacity, part_width).astype(jnp.float32)
    routed = jnp.dot(combine, back_rows, precision=lax.Precision.HIGHEST)
    return (shared_out + routed).astype(jnp.bfloat16)


def solution(mesh):
    torus = Mesh(mesh.devices.reshape(mesh.shape["ep"], 4, 4), ("ep", "tp_0", "tp_1"))
    in_specs = (
        P("ep", TP),
        P(TP),
        P("ep", None),
        P("ep", None),
        P("ep", TP, None),
        P("ep", TP, None),
        P("ep", None, TP),
        P(TP, None),
        P(TP, None),
        P(None, TP),
    )
    out_specs = P("ep", TP)
    return jax.shard_map(local, mesh=torus, in_specs=in_specs, out_specs=out_specs, check_vma=False)
```

profile of v0, /device:TPU:1, one launch (start us, length us, event | category | flops | bytes accessed | tf_op | source)
XLA Modules:
  0.0 178.6 jit_solution(14124814302274328530)
XLA Ops:
  0.0 0.0 copy-start
  0.0 0.0 copy-start.1
  0.0 0.9 fusion.11
  0.9 9.5 %psum.14 = f32[12]{0:T(128)S(1)} all-reduce(f32[12]{0:T(128)S(1)} %fusion.11), channel_id=1, replica_groups=mesh['ep'=64,'tp_0'=4,'tp_1'=4] {'tp_0'}, use_global_device_ids=true, to_apply=%region_1.0 | all-reduce | flops 12 | bytes 96 | tf_op jit(solution)/shard_map/psum | solution.py:48
  10.4 8.5 %psum.15 = f32[12]{0:T(128)S(1)} all-reduce(f32[12]{0:T(128)S(1)} %psum.14), channel_id=1, replica_groups=mesh['ep'=64,'tp_0'=4,'tp_1'=4] {'tp_1'}, use_global_device_ids=true, to_apply=%region_2.0 | all-reduce | flops 12 | bytes 96 | tf_op jit(solution)/shard_map/psum | solution.py:48
  18.9 0.8 copy.23
  19.7 0.1 eq.40
  19.8 0.1 fusion.7
  19.9 0.1 reduce_window_sum.11
  20.0 0.2 select_reduce_fusion.1
  20.1 0.1 reshape.149
  20.2 0.1 fusion.6
  20.4 0.9 convolution_convert_fusion.1
  21.3 58.6 %all_to_all.26 = bf16[64,2,256]{2,1,0:T(2,128)(2,1)S(1)} all-to-all(bf16[64,2,256]{2,1,0:T(2,128)(2,1)S(1)} %reshape.150), channel_id=1, replica_groups=mesh['ep'=64,'tp_0'=4,'tp_1'=4] {'ep'}, dimensions={0} | all-to-all | bytes 131072 | tf_op jit(solution)/shard_map/all_to_all | solution.py:116
  79.9 0.0 copy-done
  79.9 0.2 fusion.2
  80.2 0.0 copy-done.1
  80.2 0.2 fusion.4
  80.4 0.1 pad_maximum_fusion
  80.5 1.3 copy.26
  81.9 0.0 copy-start.2
  81.9 0.0 copy-start.6
  81.9 0.0 copy-start.8
  81.9 0.0 copy-start.3
  81.9 3.8 %all-to-all-start.2 = ((f32[16,256,64]{1,2,0:T(8,128)}), f32[16,256,64]{1,2,0:T(8,128)S(1)}, u32[]{:S(2)}, u32[]{:S(2)}) async-start(f32[16,256,64]{1,2,0:T(8,128)} %bitcast.3), calls=%async_computation.2 | async-start | bytes 2097152 | tf_op jit(solution)/shard_map/all_to_all | solution.py:19
  85.7 0.0 copy-done.2
  85.7 0.0 copy-done.6
  85.7 0.0 copy-done.8
  85.7 0.2 fusion.16
  86.0 0.0 copy-done.3
  86.0 0.2 fusion.18
  86.2 14.8 %all-to-all-done.2 = f32[16,256,64]{1,2,0:T(8,128)S(1)} async-done(((f32[16,256,64]{1,2,0:T(8,128)}), f32[16,256,64]{1,2,0:T(8,128)S(1)}, u32[]{:S(2)}, u32[]{:S(2)}) %all-to-all-start.2) | async-done | bytes 1048608 | tf_op jit(solution)/shard_map/all_to_all | solution.py:19
  101.0 2.4 %broadcast_in_dim.16 = f32[16,1,24576]{2,1,0:T(1,128)} broadcast(f32[24576]{0:T(1024)S(1)} %pad_maximum_fusion.1), dimensions={2} | broadcast | bytes 1671168 | tf_op jit(solution)/shard_map/broadcast_in_dim | solution.py:39
  103.4 0.0 copy-start.7
  103.4 4.8 %all-to-all-start = ((f32[16,1,24576]{2,1,0:T(1,128)}), f32[16,1,24576]{2,1,0:T(1,128)S(1)}, u32[]{:S(2)}, u32[]{:S(2)}) async-start(f32[16,1,24576]{2,1,0:T(1,128)} %broadcast_in_dim.16), calls=%async_computation | async-start | bytes 3145728 | tf_op jit(solution)/shard_map/all_to_all | solution.py:40
  108.2 0.0 copy-done.7
  108.2 0.1 reduce_sum.59
  108.3 0.0 copy-start.5
  108.3 20.4 %all-to-all-done = f32[16,1,24576]{2,1,0:T(1,128)S(1)} async-done(((f32[16,1,24576]{2,1,0:T(1,128)}), f32[16,1,24576]{2,1,0:T(1,128)S(1)}, u32[]{:S(2)}, u32[]{:S(2)}) %all-to-all-start) | async-done | bytes 1572896 | tf_op jit(solution)/shard_map/all_to_all | solution.py:40
  128.7 0.7 broadcast_in_dim.28
  129.5 5.6 %all-to-all-start.3 = ((bf16[16,128,64]{1,2,0:T(8,128)(2,1)}), bf16[16,128,64]{1,2,0:T(8,128)(2,1)S(1)}, u32[]{:S(2)}, u32[]{:S(2)}) async-start(bf16[16,128,64]{1,2,0:T(8,128)(2,1)} %broadcast_in_dim.28), calls=%async_computation.3 | async-start | bytes 524288 | tf_op jit(solution)/shard_map/all_to_all | solution.py:40
  135.1 0.1 copy.25
  135.2 0.1 select_reduce_fusion
  135.3 0.0 copy-start.4
  135.3 1.0 reduce_sum.55
  136.4 6.4 %all-to-all-done.3 = bf16[16,128,64]{1,2,0:T(8,128)(2,1)S(1)} async-done(((bf16[16,128,64]{1,2,0:T(8,128)(2,1)}), bf16[16,128,64]{1,2,0:T(8,128)(2,1)S(1)}, u32[]{:S(2)}, u32[]{:S(2)}) %all-to-all-start.3) | async-done | bytes 262176 | tf_op jit(solution)/shard_map/all_to_all | solution.py:40
  142.7 0.0 copy-done.5
  142.7 0.3 convolution_convert_fusion
  143.0 0.7 reshape.154
  143.7 9.0 %all-to-all-start.4 = ((bf16[64,2,256]{2,1,0:T(2,128)(2,1)}), bf16[64,2,256]{2,1,0:T(2,128)(2,1)S(1)}, u32[]{:S(2)}, u32[]{:S(2)}) async-start(bf16[64,2,256]{2,1,0:T(2,128)(2,1)} %reshape.154), calls=%async_computation.4 | async-start | bytes 131072 | tf_op jit(solution)/shard_map/all_to_all | solution.py:119
  152.7 0.0 copy-done.4
  152.8 0.2 fusion.8
  152.9 24.9 %all-to-all-done.4 = bf16[64,2,256]{2,1,0:T(2,128)(2,1)S(1)} async-done(((bf16[64,2,256]{2,1,0:T(2,128)(2,1)}), bf16[64,2,256]{2,1,0:T(2,128)(2,1)S(1)}, u32[]{:S(2)}, u32[]{:S(2)}) %all-to-all-start.4) | async-done | bytes 65568 | tf_op jit(solution)/shard_map/all_to_all | solution.py:119
  177.9 0.8 fusion
  (14 shorter events, 0.2 us)
Async XLA Ops:
  0.0 79.9 %copy-start = (bf16[1,256,1024]{2,1,0:T(8,128)(2,1)S(1)}, bf16[1,256,1024]{2,1,0:T(8,128)(2,1)}, u32[]{:S(2)}) copy-start(bf16[1,256,1024]{2,1,0:T(8,128)(2,1)} %param.15) | copy-start | bytes 1572868
  0.0 80.2 %copy-start.1 = (bf16[1,256,1024]{2,1,0:T(8,128)(2,1)S(1)}, bf16[1,256,1024]{2,1,0:T(8,128)(2,1)}, u32[]{:S(2)}) copy-start(bf16[1,256,1024]{2,1,0:T(8,128)(2,1)} %param.14) | copy-start | bytes 1572868
  81.9 3.8 %copy-start.2 = (bf16[256,1024]{1,0:T(8,128)(2,1)S(1)}, bf16[256,1024]{1,0:T(8,128)(2,1)}, u32[]{:S(2)}) copy-start(bf16[256,1024]{1,0:T(8,128)(2,1)} %param.18) | copy-start | bytes 1572868
  81.9 3.8 %copy-start.6 = (bf16[12,256]{1,0:T(8,128)(2,1)S(1)}, bf16[12,256]{1,0:T(8,128)(2,1)}, u32[]{:S(2)}) copy-start(bf16[12,256]{1,0:T(8,128)(2,1)} %param.10) | copy-start | bytes 18436
  81.9 3.8 %copy-start.8 = (f32[256]{0:T(256)S(1)}, f32[256]{0:T(256)}, u32[]{:S(2)}) copy-start(f32[256]{0:T(256)} %param.11) | copy-start | bytes 3076
  81.9 4.1 %copy-start.3 = (bf16[256,1024]{1,0:T(8,128)(2,1)S(1)}, bf16[256,1024]{1,0:T(8,128)(2,1)}, u32[]{:S(2)}) copy-start(bf16[256,1024]{1,0:T(8,128)(2,1)} %param.17) | copy-start | bytes 1572868
  81.9 19.1 %all-to-all-start.2 = ((f32[16,256,64]{1,2,0:T(8,128)}), f32[16,256,64]{1,2,0:T(8,128)S(1)}, u32[]{:S(2)}, u32[]{:S(2)}) async-start(f32[16,256,64]{1,2,0:T(8,128)} %bitcast.3), calls=%async_computation.2 | async-start | bytes 2097152 | tf_op jit(solution)/shard_map/all_to_all | solution.py:19
  103.4 4.8 %copy-start.7 = (f32[12,6]{0,1:T(8,128)S(1)}, f32[12,6]{0,1:T(8,128)}, u32[]{:S(2)}) copy-start(f32[12,6]{0,1:T(8,128)} %param.13) | copy-start | bytes 868
  103.4 25.3 %all-to-all-start = ((f32[16,1,24576]{2,1,0:T(1,128)}), f32[16,1,24576]{2,1,0:T(1,128)S(1)}, u32[]{:S(2)}, u32[]{:S(2)}) async-start(f32[16,1,24576]{2,1,0:T(1,128)} %broadcast_in_dim.16), calls=%async_computation | async-start | bytes 3145728 | tf_op jit(solution)/shard_map/all_to_all | solution.py:40
  108.3 34.4 %copy-start.5 = (bf16[1,1024,256]{2,1,0:T(8,128)(2,1)S(1)}, bf16[1,1024,256]{2,1,0:T(8,128)(2,1)}, u32[]{:S(2)}) copy-start(bf16[1,1024,256]{2,1,0:T(8,128)(2,1)} %param.16) | copy-start | bytes 1572868
  129.5 13.3 %all-to-all-start.3 = ((bf16[16,128,64]{1,2,0:T(8,128)(2,1)}), bf16[16,128,64]{1,2,0:T(8,128)(2,1)S(1)}, u32[]{:S(2)}, u32[]{:S(2)}) async-start(bf16[16,128,64]{1,2,0:T(8,128)(2,1)} %broadcast_in_dim.28), calls=%async_computation.3 | async-start | bytes 524288 | tf_op jit(solution)/shard_map/all_to_all | solution.py:40
  135.3 17.4 %copy-start.4 = (bf16[1024,256]{1,0:T(8,128)(2,1)S(1)}, bf16[1024,256]{1,0:T(8,128)(2,1)}, u32[]{:S(2)}) copy-start(bf16[1024,256]{1,0:T(8,128)(2,1)} %param.19) | copy-start | bytes 1572868
  143.7 34.2 %all-to-all-start.4 = ((bf16[64,2,256]{2,1,0:T(2,128)(2,1)}), bf16[64,2,256]{2,1,0:T(2,128)(2,1)S(1)}, u32[]{:S(2)}, u32[]{:S(2)}) async-start(bf16[64,2,256]{2,1,0:T(2,128)(2,1)} %reshape.154), calls=%async_computation.4 | async-start | bytes 131072 | tf_op jit(solution)/shard_map/all_to_all | solution.py:119
where the time goes:
time: 179 us
  blocking collectives  76.6 us (43%)
  waiting for transfers between devices  66.5 us (37%)
  starting transfers between devices  23.2 us (13%)
  local copies, waits for them, and re-layouts  6.34 us (4%)
  matrix products  3.02 us (2%)
  other arithmetic  2.74 us (2%)
    all_to_all x1, blocking collectives, local(): lax.all_to_all(outgoing, 'ep', split_axis=0, concat_axis=0, tiled=True)  58.6 us
    all_to_all x2, waiting for transfers between devices, sent_to_all(): return lax.all_to_all(copies, axis, split_axis=0, concat_axis=0, tiled=True)  26.8 us
    all_to_all x1, waiting for transfers between devices, local(): back = lax.all_to_all(result, 'ep', split_axis=0, concat_axis=0, tiled=True)  24.9 us
    psum x2, blocking collectives, one_axis_at_a_time(): return functools.reduce(lax.psum, axes, x)  18 us
    all_to_all x1, waiting for transfers between devices, summed_on_arrival(): lax.all_to_all(tiles, axis, split_axis=0, concat_axis=0, tiled=True)  14.8 us
    all_to_all x2, starting transfers between devices, sent_to_all(): return lax.all_to_all(copies, axis, split_axis=0, concat_axis=0, tiled=True)  10.4 us
    all_to_all x1, starting transfers between devices, local(): back = lax.all_to_all(result, 'ep', split_axis=0, concat_axis=0, tiled=True)  9.02 us
    all_to_all x1, starting transfers between devices, summed_on_arrival(): lax.all_to_all(tiles, axis, split_axis=0, concat_axis=0, tiled=True)  3.8 us
  transfers between devices with their start and end apart: 4, of which 4 were waited for; matrix products, arithmetic and copies ran while one was open for 1% of the time, Pallas kernels for 0%

commit v1 on v0

v1 whole, which is shorter than its diff:
```python
import functools

import jax
import jax.numpy as jnp
from jax import lax
from jax.experimental import pallas as pl
from jax.experimental.pallas import tpu as pltpu
from jax.sharding import Mesh
from jax.sharding import PartitionSpec as P

MESH = pl.DeviceIdType.MESH
F32 = jnp.float32
BF16 = jnp.bfloat16
DOWN_SCALE = 2.0**-40
UP_SCALE = 2.0**40


def silu(v):
    return v / (1.0 + jnp.exp(-v))


def row_of(col, width):
    rows = col.shape[0]
    eye = lax.broadcasted_iota(jnp.int32, (rows, width), 0) == lax.broadcasted_iota(
        jnp.int32, (rows, width), 1
    )
    return jnp.sum(jnp.where(eye, col, 0.0), axis=0, keepdims=True)


def col_of(row, rows, first):
    width = row.shape[1]
    eye = lax.broadcasted_iota(jnp.int32, (rows, width), 0) + first == lax.broadcasted_iota(
        jnp.int32, (rows, width), 1
    )
    return jnp.sum(jnp.where(eye, row, 0.0), axis=1, keepdims=True)


def kernel(
    sizes,
    tok_hbm,
    gain_hbm,
    routes_hbm,
    weights_hbm,
    eg_hbm,
    eu_hbm,
    ed_hbm,
    sg_hbm,
    su_hbm,
    sd_hbm,
    out_ref,
    tok,
    gain,
    routes,
    weights,
    eg,
    eu,
    ed,
    sg,
    su,
    sd,
    tok16,
    routes16,
    weights16,
    slotw,
    shared_out,
    msg,
    relay_p,
    relay_m,
    rx,
    sq_tx,
    sq_rx,
    sqs_tx,
    sqs_rx,
    part_tx,
    part_rx,
    spart_tx,
    spart_rx,
    hid_tx,
    hid,
    shid_tx,
    shid,
    ret,
    back,
    load_sem,
    disp_send,
    disp_recv,
    rel_send,
    rel_recv,
    tp_send,
    sq_recv,
    part_recv,
    hid_recv,
    ret_send,
    ret_recv,
):
    nz, ny, nx, hop = sizes
    ntp = ny * nx
    half_z = nz // 2
    tok_n, picks = routes.shape
    width = tok.shape[1]
    total_width = float(width * ntp)
    slots = 4 * nz
    rows = slots // 2
    half = rows // 2
    ff = eg.shape[1]
    chunk = ff // (ntp // 2)
    n_plus, n_minus = half_z - 1 - hop, half_z - hop

    z, c = lax.axis_index("z"), lax.axis_index("c")
    y, x = lax.axis_index("y"), lax.axis_index("x")
    me = y * nx + x
    my_half, my_chunk = lax.rem(me, 2), me // 2

    def at(d):
        return lax.rem(z + d + 2 * nz, nz)

    def peer(i):
        j = lax.rem(me + i, ntp)
        return j, (z, c, j // nx, lax.rem(j, nx))

    loads = []
    for i, (src, dst) in enumerate(
        (
            (tok_hbm, tok),
            (routes_hbm, routes),
            (weights_hbm, weights),
            (gain_hbm, gain),
            (sg_hbm, sg),
            (su_hbm, su),
            (eg_hbm.at[0], eg),
            (eu_hbm.at[0], eu),
            (sd_hbm, sd),
            (ed_hbm.at[0], ed),
        )
    ):
        copy = pltpu.make_async_copy(src, dst, load_sem.at[i])
        copy.start()
        loads.append(copy)

    barrier = pltpu.get_barrier_semaphore()

    def greet_z(d, carry):
        for core in range(2):
            pl.semaphore_signal(barrier, inc=1, device_id=(at(d), core, y, x), device_id_type=MESH)
            pl.semaphore_signal(barrier, inc=1, device_id=(at(-d), core, y, x), device_id_type=MESH)
        return carry

    def greet_tp(i, carry):
        pl.semaphore_signal(barrier, inc=1, device_id=peer(i)[1], device_id_type=MESH)
        return carry

    lax.fori_loop(1, hop + 1, greet_z, 0)
    pl.semaphore_signal(barrier, inc=1, device_id=(z, 1 - c, y, x), device_id_type=MESH)
    lax.fori_loop(1, ntp, greet_tp, 0)

    tok16[...] = jnp.zeros_like(tok16)
    routes16[...] = jnp.full_like(routes16, -1)
    weights16[...] = jnp.ones_like(weights16)
    for i in range(4):
        loads[i].wait()
    tok16[0:tok_n, :] = tok[...]
    routes16[0:tok_n, :] = routes[...]
    weights16[0:tok_n, :] = weights[...]
    picked, affinity = routes16[...], weights16[...]
    lane = lax.broadcasted_iota(jnp.int32, (16, slots), 1)
    chip = lane // 4 + (z + half_z)
    chip = jnp.where(chip >= nz, chip - nz, chip)
    chip = jnp.where(chip >= nz, chip - nz, chip)
    expert = chip * 2 + (lane // 2) % 2
    scaled = 2.5 * affinity / jnp.sum(affinity, axis=1, keepdims=True)
    named = jnp.zeros((16, slots), F32)
    weight = jnp.zeros((16, slots), F32)
    for k in range(picks):
        hit = picked[:, k : k + 1] == expert
        named = jnp.where(hit, 1.0, named)
        weight = jnp.where(hit, scaled[:, k : k + 1], weight)
    earlier = (
        lax.broadcasted_iota(jnp.int32, (16, 16), 1) < lax.broadcasted_iota(jnp.int32, (16, 16), 0)
    ).astype(F32)
    before = jnp.dot(earlier, named, preferred_element_type=F32)
    rank = (lane % 2).astype(F32)
    select = jnp.where(before == rank, named, 0.0)
    slotw[...] = jnp.where(before == rank, weight, 0.0)
    tokens16 = tok16[...]
    outgoing = lax.dot_general(
        select.astype(BF16), tokens16, (((0,), (0,)), ((), ())), preferred_element_type=F32
    ).astype(BF16)
    for i in range(slots // 2):
        msg[i] = outgoing[2 * i : 2 * i + 2, :]

    gains = gain[...] * DOWN_SCALE
    values = tokens16.astype(F32)
    scaled_tok = (values * gains).astype(BF16)
    sqs_tx[...] = row_of(jnp.sum(values * values, axis=1, keepdims=True), 128)
    sqs_rx[me] = sqs_tx[...]

    pl.semaphore_wait(barrier, 4 * hop + 1 + ntp - 1)

    def bundle(first, count, landing, target, k):
        return pltpu.make_async_remote_copy(
            src_ref=msg.at[pl.ds(first, count)],
            dst_ref=landing.at[:, c],
            send_sem=disp_send,
            recv_sem=rel_recv.at[k],
            device_id=(target, 1, y, x),
            device_id_type=MESH,
        )

    bundle(2 * (half_z + hop + 1), 2 * n_plus, relay_p, at(hop), 0).start()
    bundle(0, 2 * n_minus, relay_m, at(-hop), 1).start()

    def place(d):
        p = lax.rem(hop - d + 2 * nz, nz)
        return p // half_z, lax.rem(p, half_z)

    def send_near(d, core):
        group, p = place(d)
        pltpu.make_async_remote_copy(
            src_ref=msg.at[2 * (d + half_z) + core],
            dst_ref=rx.at[group, 2 * p + c],
            send_sem=disp_send,
            recv_sem=disp_recv.at[group],
            device_id=(at(d), core, y, x),
            device_id_type=MESH,
        ).start()

    def near(i, carry):
        d = hop - i
        for core in range(2):
            send_near(d, core)
            send_near(-d, core)
        return carry

    lax.fori_loop(0, hop, near, 0)
    send_near(0, 1 - c)
    g0, p0 = place(0)
    rx[g0, 2 * p0 + c] = msg[2 * half_z + c]

    def to_tp(src, dst, recv):
        def one(i, carry):
            j, device = peer(i)
            pltpu.make_async_remote_copy(
                src_ref=src(j),
                dst_ref=dst,
                send_sem=tp_send,
                recv_sem=recv,
                device_id=device,
                device_id_type=MESH,
            ).start()
            return carry

        lax.fori_loop(1, ntp, one, 0)

    def waiting(src, dst, send, recv):
        return pltpu.make_async_remote_copy(
            src_ref=src,
            dst_ref=dst,
            send_sem=send,
            recv_sem=recv,
            device_id=peer(1)[1],
            device_id_type=MESH,
        )

    to_tp(lambda j: sqs_tx, sqs_rx.at[me], sq_recv.at[2])
    for i in (4, 5):
        loads[i].wait()
    for n, w in enumerate((sg, su)):
        part = jnp.dot(scaled_tok, w[...], preferred_element_type=F32)
        for k in range(ntp // 2):
            for h in range(2):
                spart_tx[2 * k + h, n] = part[8 * h : 8 * h + 8, k * chunk : (k + 1) * chunk]
    to_tp(lambda j: spart_tx.at[j], spart_rx.at[me], part_recv.at[2])
    spart_rx[me] = spart_tx[me]

    @pl.when(c == 1)
    def _():
        waiting(relay_p, relay_p, rel_send, rel_recv.at[0]).wait_recv()

        def forward_plus(i, carry):
            for core in range(2):
                group, p = place(i + hop + 1)
                pltpu.make_async_remote_copy(
                    src_ref=relay_p.at[2 * i + core],
                    dst_ref=rx.at[group, pl.ds(2 * p, 2)],
                    send_sem=rel_send,
                    recv_sem=disp_recv.at[group],
                    device_id=(at(i + 1), core, y, x),
                    device_id_type=MESH,
                ).start()
            return carry

        lax.fori_loop(0, n_plus, forward_plus, 0)
        waiting(relay_m, relay_m, rel_send, rel_recv.at[1]).wait_recv()

        def forward_minus(i, carry):
            for core in range(2):
                group, p = place(i - half_z)
                pltpu.make_async_remote_copy(
                    src_ref=relay_m.at[2 * i + core],
                    dst_ref=rx.at[group, pl.ds(2 * p, 2)],
                    send_sem=rel_send,
                    recv_sem=disp_recv.at[group],
                    device_id=(at(i - half_z + hop), core, y, x),
                    device_id_type=MESH,
                ).start()
            return carry

        lax.fori_loop(0, n_minus, forward_minus, 0)

    def gate_up(group):
        count = 2 * half_z - (1 if group == 0 else 0)
        arrived = rx.at[group, pl.ds(0, count)]
        waiting(arrived, arrived, disp_send, disp_recv.at[group]).wait_recv()
        values = rx[group].reshape(rows, width).astype(F32)
        sq_tx[group] = row_of(jnp.sum(values * values, axis=1, keepdims=True), 128)
        sq_rx[group, me] = sq_tx[group]
        to_tp(lambda j: sq_tx.at[group], sq_rx.at[group, me], sq_recv.at[group])
        lhs = (values * gains).astype(BF16)
        for n, w in enumerate((eg, eu)):
            part = jnp.dot(lhs, w[...], preferred_element_type=F32).astype(BF16)
            for k in range(ntp // 2):
                for h in range(2):
                    part_tx[group, 2 * k + h, n] = part[
                        half * h : half * (h + 1), k * chunk : (k + 1) * chunk
                    ]
        to_tp(lambda j: part_tx.at[group, j], part_rx.at[group, me], part_recv.at[group])
        part_rx[group, me] = part_tx[group, me]

    def hidden_of(squares, parts, n):
        total = jnp.zeros((1, 128), F32)
        gate = jnp.zeros((n, chunk), F32)
        up = jnp.zeros((n, chunk), F32)
        for j in range(ntp):
            total = total + squares[j]
            gate = gate + parts[j, 0].astype(F32)
            up = up + parts[j, 1].astype(F32)
        inv = lax.rsqrt(total / total_width + 1e-06) * UP_SCALE
        inv = col_of(inv, n, my_half * n)
        return (silu(gate * inv) * (up * inv)).astype(BF16)

    def tp_wait(buf, recv):
        some = buf.at[pl.ds(0, ntp - 1)]
        waiting(some, some, tp_send, recv).wait_recv()

    columns = pl.ds(pl.multiple_of(my_chunk * chunk, chunk), chunk)

    def reduce_group(group):
        tp_wait(sq_rx.at[group], sq_recv.at[group])
        tp_wait(part_rx.at[group], part_recv.at[group])
        hid_tx[group] = hidden_of(sq_rx.at[group], part_rx.at[group], half)
        own = hid.at[group, pl.ds(pl.multiple_of(my_half * half, half), half), columns]
        own[...] = hid_tx[group]
        to_tp(lambda j: hid_tx.at[group], own, hid_recv.at[group])

    def reduce_shared():
        tp_wait(sqs_rx, sq_recv.at[2])
        tp_wait(spart_rx, part_recv.at[2])
        shid_tx[...] = hidden_of(sqs_rx, spart_rx, 8)
        own = shid.at[my_half, :, columns]
        own[...] = shid_tx[...]
        to_tp(lambda j: shid_tx, own, hid_recv.at[2])

    def down_shared():
        waiting(spart_half, spart_half, tp_send, hid_recv.at[2]).wait_recv()
        loads[8].wait()
        total = jnp.zeros((16, width), F32)
        hidden = jnp.concatenate([shid[0], shid[1]], axis=0)
        shared_out[...] = total + jnp.dot(hidden, sd[...], preferred_element_type=F32)

    spart_half = part_rx.at[0, pl.ds(0, ntp - 1), 0, pl.ds(0, 8)]

    def down(group):
        blocks = part_rx.at[group, pl.ds(0, ntp - 1), 0]
        waiting(blocks, blocks, tp_send, hid_recv.at[group]).wait_recv()
        result = jnp.dot(hid[group], ed[...], preferred_element_type=F32).astype(BF16)
        for i in range(rows // 2):
            ret[group, i] = result[2 * i : 2 * i + 2, :]

        def give_back(p):
            s = p - hop
            place_there = 2 * lax.rem(half_z - s + 2 * nz, nz) + c
            for core in range(2):
                pltpu.make_async_remote_copy(
                    src_ref=ret.at[group, 2 * (p - group * half_z) + core],
                    dst_ref=back.at[place_there],
                    send_sem=ret_send,
                    recv_sem=ret_recv,
                    device_id=(at(s), core, y, x),
                    device_id_type=MESH,
                ).start()

        if group == 0:

            def outer(i, carry):
                give_back(i)
                give_back(half_z - 1 - i)
                return carry

            lax.fori_loop(0, hop - 1, outer, 0)
            give_back(hop - 1)
            pltpu.make_async_remote_copy(
                src_ref=ret.at[0, 2 * hop + 1 - c],
                dst_ref=back.at[2 * half_z + c],
                send_sem=ret_send,
                recv_sem=ret_recv,
                device_id=(z, 1 - c, y, x),
                device_id_type=MESH,
            ).start()
            back[2 * half_z + c] = ret[0, 2 * hop + c]
        else:
            farthest = half_z + hop

            def inner(i, carry):
                give_back(farthest - i)
                give_back(farthest + 1 + i)
                return carry

            give_back(half_z)
            lax.fori_loop(0, hop - 1, inner, 0)
            give_back(half_z + 1)

    for i in (6, 7):
        loads[i].wait()
    gate_up(0)
    reduce_shared()
    gate_up(1)
    reduce_group(0)
    down_shared()
    loads[9].wait()
    reduce_group(1)
    down(0)
    down(1)

    got = back.at[pl.ds(0, 2 * nz - 1)]
    waiting(got, got, ret_send, ret_recv).wait_recv()
    rows_back = back[...].reshape(slots, width).astype(F32)
    routed = jnp.dot(
        slotw[...], rows_back, precision=lax.Precision.HIGHEST, preferred_element_type=F32
    )
    out_ref[...] = (shared_out[...] + routed)[0:tok_n, :].astype(BF16)

    def left(ref, sem):
        waiting(ref, ref, sem, ret_recv).wait_send()

    left(got, ret_send)
    left(msg.at[pl.ds(0, 2 * (n_plus + n_minus))], disp_send)
    left(msg.at[pl.ds(0, 4 * hop + 1)], disp_send)

    @pl.when(c == 1)
    def _():
        left(relay_p, rel_send)
        left(relay_m, rel_send)

    left(sqs_rx.at[pl.ds(0, ntp - 1)], tp_send)
    left(spart_rx.at[pl.ds(0, ntp - 1)], tp_send)
    left(spart_half, tp_send)
    for group in range(2):
        left(sq_rx.at[group, pl.ds(0, ntp - 1)], tp_send)
        left(part_rx.at[group, pl.ds(0, ntp - 1)], tp_send)
        left(part_rx.at[group, pl.ds(0, ntp - 1), 0], tp_send)


def local(sizes, tokens, norm_gain, routes, route_weights, eg, eu, ed, sg, su, sd):
    nz, ny, nx, hop = sizes
    ntp = ny * nx
    tok_n, width = tokens.shape
    picks = routes.shape[1]
    ff = eg.shape[2]
    chunk = ff // (ntp // 2)
    slots = 4 * nz
    rows = slots // 2
    half = rows // 2
    n_plus, n_minus = nz // 2 - 1 - hop, nz // 2 - hop
    vm = pltpu.VMEM
    scratch = [
        vm((tok_n, width), BF16),
        vm((1, width), F32),
        vm((tok_n, picks), jnp.int32),
        vm((tok_n, picks), F32),
        vm((width, ff), BF16),
        vm((width, ff), BF16),
        vm((ff, width), BF16),
        vm((width, ff), BF16),
        vm((width, ff), BF16),
        vm((ff, width), BF16),
        vm((16, width), BF16),
        vm((16, picks), jnp.int32),
        vm((16, picks), F32),
        vm((16, slots), F32),
        vm((16, width), F32),
        vm((slots // 2, 2, width), BF16),
        vm((2 * n_plus, 2, 2, width), BF16),
        vm((2 * n_minus, 2, 2, width), BF16),
        vm((2, rows // 2, 2, width), BF16),
        vm((2, 1, 128), F32),
        vm((2, ntp, 1, 128), F32),
        vm((1, 128), F32),
        vm((ntp, 1, 128), F32),
        vm((2, ntp, 2, half, chunk), BF16),
        vm((2, ntp, 2, half, chunk), BF16),
        vm((ntp, 2, 8, chunk), F32),
        vm((ntp, 2, 8, chunk), F32),
        vm((2, half, chunk), BF16),
        vm((2, rows, ff), BF16),
        vm((8, chunk), BF16),
        vm((2, 8, ff), BF16),
        vm((2, rows // 2, 2, width), BF16),
        vm((slots // 2, 2, width), BF16),
        pltpu.SemaphoreType.DMA((10,)),
        pltpu.SemaphoreType.DMA,
        pltpu.SemaphoreType.DMA((2,)),
        pltpu.SemaphoreType.DMA,
        pltpu.SemaphoreType.DMA((2,)),
        pltpu.SemaphoreType.DMA,
        pltpu.SemaphoreType.DMA((3,)),
        pltpu.SemaphoreType.DMA((3,)),
        pltpu.SemaphoreType.DMA((3,)),
        pltpu.SemaphoreType.DMA,
        pltpu.SemaphoreType.DMA,
    ]
    return pl.pallas_call(
        functools.partial(kernel, sizes),
        out_shape=jax.ShapeDtypeStruct((tok_n, width), BF16),
        in_specs=[pl.BlockSpec(memory_space=pl.ANY)] * 10,
        out_specs=pl.BlockSpec(memory_space=pltpu.VMEM),
        scratch_shapes=scratch,
        compiler_params=pltpu.CompilerParams(collective_id=0, has_side_effects=True),
        name="moe_step",
    )(tokens, norm_gain.reshape(1, width), routes, route_weights, eg, eu, ed, sg, su, sd)


def on_torus(torus):
    n = torus.shape
    sizes = (n["z"], n["y"], n["x"], n["z"] // 4)
    ep, tp = ("z", "c"), ("y", "x")
    in_specs = (
        P(ep, tp),
        P(tp),
        P(ep, None),
        P(ep, None),
        P(ep, tp, None),
        P(ep, tp, None),
        P(ep, None, tp),
        P(tp, None),
        P(tp, None),
        P(None, tp),
    )
    return jax.shard_map(
        functools.partial(local, sizes),
        mesh=torus,
        in_specs=in_specs,
        out_specs=P(ep, tp),
        check_vma=False,
    )


def solution(mesh):
    return on_torus(Mesh(mesh.devices.reshape(32, 2, 4, 4), ("z", "c", "y", "x")))
```

time: 179 us -> 69.4 us (0.39)
  blocking collectives: 76.6 us -> 0 us
  waiting for transfers between devices: 66.5 us -> 0 us
  Pallas kernels: 0 us -> 65.7 us
  starting transfers between devices: 23.2 us -> 0 us
  matrix products: 3.02 us -> 0 us
  local copies, waits for them, and re-layouts: 6.34 us -> 3.35 us
  other arithmetic: 2.74 us -> 0 us
    all_to_all x4 -> x0, waiting for transfers between devices: 66.5 us -> none  [the longest x2 26.8 us: sent_to_all(): return lax.all_to_all(copies, axis, split_axis=0, concat_axis=0, tiled=True)]
    pallas_call x0 -> x1, Pallas kernels: none -> 65.7 us  [local(): pl.pallas_call(functools.partial(kernel, sizes), out_shape=jax.ShapeDtype...]
    all_to_all x1 -> x0, blocking collectives: 58.6 us -> none  [local(): lax.all_to_all(outgoing, 'ep', split_axis=0, concat_axis=0, tiled=True)]
    all_to_all x4 -> x0, starting transfers between devices: 23.2 us -> none  [the longest x2 10.4 us: sent_to_all(): return lax.all_to_all(copies, axis, split_axis=0, concat_axis=0, tiled=True)]
    psum x2 -> x0, blocking collectives: 18 us -> none  [one_axis_at_a_time(): return functools.reduce(lax.psum, axes, x)]
    broadcast_in_dim x2 -> x0, local copies, waits for them, and re-layouts: 3.11 us -> none  [sent_to_all(): copies = jnp.broadcast_to(x, (lax.axis_size(axis), *x.shape))]
    dot_general x8 -> x0, matrix products: 3.02 us -> none  [the longest x1 0.92 us: local(): jnp.einsum('tj,td->jd', select, normed, preferred_element_type=jnp.float32)]
    unnamed x19 -> x5, local copies, waits for them, and re-layouts: 0.82 us -> 3.35 us
  transfers between devices with their start and end apart: 4 -> 0, of which waited for: 4 -> 0; matrix products, arithmetic and copies ran while one was open for 1% -> 0% of each run, Pallas kernels for 0% -> 0%
where the time goes in v1:
time: 69.4 us; the launch traced here: 69.1 us
  Pallas kernels  65.7 us (95%)
  local copies, waits for them, and re-layouts  3.35 us (5%)
    pallas_call x1, Pallas kernels, local(): pl.pallas_call(functools.partial(kernel, sizes), out_shape=jax.ShapeDtype...  65.7 us
    unnamed x5, local copies, waits for them, and re-layouts  3.35 us

profile of v1, /device:TPU:1, one launch (start us, length us, event | category | flops | bytes accessed | tf_op | source)
XLA Modules:
  0.0 69.1 jit_solution(14381588980796582720)
XLA Ops:
  0.0 0.0 copy-start
  0.0 1.4 %copy.11.routes_hbm = s32[12,6]{1,0:T(8,128)} copy(s32[12,6]{0,1:T(8,128)} %param.12) | data formatting | bytes 576 | tf_op args[2]
  1.4 0.0 copy-done
  1.4 0.7 copy.12.weights_hbm
  2.1 65.7 %moe_step.1 = bf16[12,256]{1,0:T(8,128)(2,1)} custom-call(bf16[12,256]{1,0:T(8,128)(2,1)} %tok_hbm.1, f32[1,256]{1,0:T(1,128)} %bitcast.1, s32[12,6]{1,0:T(8,128)} %copy.11.routes_hbm, f32[12,6]{1,0:T(8,128)} %copy.12.weights_hbm, bf16[1,256,1024]{2,1,0:T(8,128)(2,1)} %eg_hbm.1, bf16[1,256,1024]{2,1,0:T(8,128)(2,1)} %eu_hbm.1, bf16[1,1024,256]{2,1,0:T(8,128)(2,1)} %ed_hbm.1, ...), custom_call_target="tpu_custom_call" | custom-call | tf_op jit(solution)/shard_map/moe_step/pallas_call | solution.py:521
  67.8 1.3 %copy.14 = bf16[12,256]{1,0:T(8,128)(2,1)} copy(bf16[12,256]{1,0:T(8,128)(2,1)} %moe_step.1) | data formatting | bytes 12288
Async XLA Ops:
  0.0 1.4 %copy-start = (f32[12,6]{0,1:T(8,128)S(1)}, f32[12,6]{0,1:T(8,128)}, u32[]{:S(2)}) copy-start(f32[12,6]{0,1:T(8,128)} %param.13) | copy-start | bytes 868

commit v2 on v1

v2 whole, which is shorter than its diff:
```python
import functools

import jax
import jax.numpy as jnp
from jax import lax
from jax.experimental import pallas as pl
from jax.experimental.pallas import tpu as pltpu
from jax.sharding import Mesh
from jax.sharding import PartitionSpec as P

MESH = pl.DeviceIdType.MESH
F32 = jnp.float32
BF16 = jnp.bfloat16
DOWN_SCALE = 2.0**-40
UP_SCALE = 2.0**40


def silu(v):
    return v / (1.0 + jnp.exp(-v))


def row_of(col, width):
    rows = col.shape[0]
    eye = lax.broadcasted_iota(jnp.int32, (rows, width), 0) == lax.broadcasted_iota(
        jnp.int32, (rows, width), 1
    )
    return jnp.sum(jnp.where(eye, col, 0.0), axis=0, keepdims=True)


def col_of(row, rows, first):
    width = row.shape[1]
    eye = lax.broadcasted_iota(jnp.int32, (rows, width), 0) + first == lax.broadcasted_iota(
        jnp.int32, (rows, width), 1
    )
    return jnp.sum(jnp.where(eye, row, 0.0), axis=1, keepdims=True)


def rings(nz):
    return (0, nz // 4, nz // 2, nz)


def kernel(
    sizes,
    tok_hbm,
    gain_hbm,
    routes_hbm,
    weights_hbm,
    eg_hbm,
    eu_hbm,
    ed_hbm,
    sg_hbm,
    su_hbm,
    sd_hbm,
    out_ref,
    tok,
    gain,
    routes,
    weights,
    eg,
    eu,
    ed,
    sg,
    su,
    sd,
    tok16,
    routes16,
    weights16,
    slotw,
    shared_out,
    msg,
    relay_p,
    relay_m,
    rx,
    sq_tx,
    sq_rx,
    spart_tx,
    spart_rx,
    shid_tx,
    shid,
    hid,
    ret,
    back,
    part_tx,
    part_rx,
    hid_tx,
    load_sem,
    disp_send,
    disp_recv,
    rel_send,
    rel_recv,
    tp_send,
    sq_recv,
    part_recv,
    hid_recv,
    ret_send,
    ret_recv,
    entered,
):
    nz, ny, nx, hop = sizes
    ntp = ny * nx
    half_z = nz // 2
    ends = rings(nz)
    groups = len(ends) - 1
    close = hop // 2
    picks, tok_n = routes.shape
    width = tok.shape[1]
    total_width = float(width * ntp)
    slots = 4 * nz
    ff = eg.shape[1]
    chunk = ff // (ntp // 2)
    n_plus, n_minus = half_z - hop, half_z - 1 - hop
    least = 1 - half_z

    z, c = lax.axis_index("z"), lax.axis_index("c")
    y, x = lax.axis_index("y"), lax.axis_index("x")
    me = y * nx + x
    my_half, my_chunk = lax.rem(me, 2), me // 2

    def at(d):
        return lax.rem(z + d + 2 * nz, nz)

    def peer(i):
        j = lax.rem(me + i, ntp)
        return j, (z, c, j // nx, lax.rem(j, nx))

    barrier = pltpu.get_barrier_semaphore()

    def greet_z(i, carry):
        for core in range(2):
            for d in (close - i, i - close):
                pl.semaphore_signal(
                    barrier, inc=1, device_id=(at(d), core, y, x), device_id_type=MESH
                )
        return carry

    def greet_tp(i, carry):
        pl.semaphore_signal(barrier, inc=1, device_id=peer(i)[1], device_id_type=MESH)
        return carry

    lax.fori_loop(0, close, greet_z, 0)
    pl.semaphore_signal(barrier, inc=1, device_id=(z, 1 - c, y, x), device_id_type=MESH)
    lax.fori_loop(1, ntp, greet_tp, 0)

    loads = []
    for i, (src, dst) in enumerate(
        (
            (tok_hbm, tok),
            (routes_hbm, routes),
            (weights_hbm, weights),
            (gain_hbm, gain),
            (sg_hbm, sg),
            (su_hbm, su),
            (eg_hbm.at[0], eg),
            (eu_hbm.at[0], eu),
            (sd_hbm, sd),
            (ed_hbm.at[0], ed),
        )
    ):
        copy = pltpu.make_async_copy(src, dst, load_sem.at[i])
        copy.start()
        loads.append(copy)

    tok16[...] = jnp.zeros_like(tok16)
    routes16[...] = jnp.full_like(routes16, -1)
    weights16[...] = jnp.ones_like(weights16)
    for i in range(4):
        loads[i].wait()
    tok16[0:tok_n, :] = tok[...]
    routes16[:, 0:tok_n] = routes[...]
    weights16[:, 0:tok_n] = weights[...]
    picked, affinity = routes16[...], weights16[...]
    slot = lax.broadcasted_iota(jnp.int32, (slots, 16), 0)
    chip = slot // 4 + (z + nz + least)
    chip = jnp.where(chip >= nz, chip - nz, chip)
    chip = jnp.where(chip >= nz, chip - nz, chip)
    expert = chip * 2 + (slot // 2) % 2
    scaled = 2.5 * affinity / jnp.sum(affinity, axis=0, keepdims=True)
    named = jnp.zeros((slots, 16), F32)
    weight = jnp.zeros((slots, 16), F32)
    for k in range(picks):
        hit = picked[k : k + 1, :] == expert
        named = jnp.where(hit, 1.0, named)
        weight = jnp.where(hit, scaled[k : k + 1, :], weight)
    earlier = (
        lax.broadcasted_iota(jnp.int32, (16, 16), 0) < lax.broadcasted_iota(jnp.int32, (16, 16), 1)
    ).astype(F32)
    before = jnp.dot(named, earlier, preferred_element_type=F32)
    rank = (slot % 2).astype(F32)
    select = jnp.where(before == rank, named, 0.0)
    slot_weight = jnp.where(before == rank, weight, 0.0)
    tokens16 = tok16[...]
    outgoing = jnp.dot(select.astype(BF16), tokens16, preferred_element_type=F32).astype(BF16)
    for i in range(slots // 2):
        msg[i] = outgoing[2 * i : 2 * i + 2, :]

    with jax.named_scope("w_barrier"):
        pl.semaphore_wait(barrier, 4 * close + 1 + ntp - 1)

    def tell(sem, d, core):
        pl.semaphore_signal(sem, inc=1, device_id=(at(d), core, y, x), device_id_type=MESH)

    tell(entered.at[0], -close, c)
    tell(entered.at[1], close, c)

    def bundle(first, count, landing, target, k):
        return pltpu.make_async_remote_copy(
            src_ref=msg.at[pl.ds(2 * (first - least), 2 * count)],
            dst_ref=landing.at[:, c],
            send_sem=disp_send,
            recv_sem=rel_recv.at[k],
            device_id=(target, 1, y, x),
            device_id_type=MESH,
        )

    def ring(source):
        return source // ends[1] - source // (3 * ends[1])

    def send_near(d, core):
        pltpu.make_async_remote_copy(
            src_ref=msg.at[2 * (d - least) + core],
            dst_ref=rx.at[2 * z + c],
            send_sem=disp_send,
            recv_sem=disp_recv.at[ring(z)],
            device_id=(at(d), core, y, x),
            device_id_type=MESH,
        ).start()

    def near_plus(i, carry):
        for core in range(2):
            send_near(hop - i, core)
        return carry

    def near_minus(i, carry):
        for core in range(2):
            send_near(i - hop, core)
        return carry

    with jax.named_scope("w_plus"):
        pl.semaphore_wait(entered.at[0], 1)
    bundle(hop + 1, n_plus, relay_p, at(hop), 0).start()
    lax.fori_loop(0, hop, near_plus, 0)
    with jax.named_scope("w_minus"):
        pl.semaphore_wait(entered.at[1], 1)
    bundle(least, n_minus, relay_m, at(-hop), 1).start()

    @pl.when(c == 1)
    def _():
        tell(entered.at[2], -hop, 1)
        tell(entered.at[3], hop, 1)

    lax.fori_loop(0, hop, near_minus, 0)
    send_near(0, 1 - c)
    rx[2 * z + c] = msg[c - 2 * least]

    def to_tp(src, dst, recv):
        def one(i, carry):
            j, device = peer(i)
            pltpu.make_async_remote_copy(
                src_ref=src(j),
                dst_ref=dst,
                send_sem=tp_send,
                recv_sem=recv,
                device_id=device,
                device_id_type=MESH,
            ).start()
            return carry

        lax.fori_loop(1, ntp, one, 0)

    def waiting(src, dst, send, recv):
        return pltpu.make_async_remote_copy(
            src_ref=src,
            dst_ref=dst,
            send_sem=send,
            recv_sem=recv,
            device_id=peer(1)[1],
            device_id_type=MESH,
        )

    gains = gain[...] * DOWN_SCALE
    values = tokens16.astype(F32)
    scaled_tok = (values * gains).astype(BF16)
    sq_tx[groups] = row_of(jnp.sum(values * values, axis=1, keepdims=True), 128)
    sq_rx[groups, me] = sq_tx[groups]
    for i in (4, 5):
        loads[i].wait()
    for n, w in enumerate((sg, su)):
        part = jnp.dot(scaled_tok, w[...], preferred_element_type=F32)
        for k in range(ntp // 2):
            for h in range(2):
                spart_tx[2 * k + h, n] = part[8 * h : 8 * h + 8, k * chunk : (k + 1) * chunk]
    spart_rx[me] = spart_tx[me]

    to_tp(lambda j: sq_tx.at[groups], sq_rx.at[groups, me], sq_recv.at[groups])
    slot_weight = slot_weight.T
    for i in range(3):
        term = slot_weight.astype(BF16)
        slotw[16 * i : 16 * i + 16, :] = term
        slot_weight = slot_weight - term.astype(F32)
    to_tp(lambda j: spart_tx.at[j], spart_rx.at[me], part_recv.at[groups])

    def forward(landing, i, source, first):
        for core in range(2):
            pltpu.make_async_remote_copy(
                src_ref=landing.at[2 * i + core],
                dst_ref=rx.at[pl.ds(2 * source, 2)],
                send_sem=rel_send,
                recv_sem=disp_recv.at[ring(source)],
                device_id=(at(first + i), core, y, x),
                device_id_type=MESH,
            ).start()

    @pl.when(c == 1)
    def _():
        with jax.named_scope("w_entered"):
            pl.semaphore_wait(entered.at[2], 1)
        with jax.named_scope("w_relp"):
            waiting(relay_p, relay_p, rel_send, rel_recv.at[0]).wait_recv()

        def forward_plus(k, carry):
            forward(relay_p, n_plus - 1 - k, at(-hop), 1)
            return carry

        lax.fori_loop(0, n_plus, forward_plus, 0)
        pl.semaphore_wait(entered.at[3], 1)
        with jax.named_scope("w_relm"):
            waiting(relay_m, relay_m, rel_send, rel_recv.at[1]).wait_recv()

        def forward_minus(i, carry):
            forward(relay_m, i, at(hop), hop + least)
            return carry

        lax.fori_loop(0, n_minus, forward_minus, 0)

    def gate_up(group):
        first, last = 2 * ends[group], 2 * ends[group + 1]
        rows = 2 * (last - first)
        half = rows // 2
        mine = ring(z) == group
        with jax.named_scope(f"w_rows{group}"):
            for count, there in ((last - first - 1, mine), (last - first, jnp.logical_not(mine))):
                arrived = rx.at[pl.ds(first, count)]

                @pl.when(there)
                def _():
                    waiting(arrived, arrived, disp_send, disp_recv.at[group]).wait_recv()

        values = rx[first:last].reshape(rows, width).astype(F32)
        lhs = (values * gains).astype(BF16)
        for n, w in enumerate((eg, eu)):
            part = jnp.dot(lhs, w[...], preferred_element_type=F32).astype(BF16)
            for k in range(ntp // 2):
                for h in range(2):
                    part_tx[group][2 * k + h, n] = part[
                        half * h : half * (h + 1), k * chunk : (k + 1) * chunk
                    ]
        sq_tx[group] = row_of(jnp.sum(values * values, axis=1, keepdims=True), 128)

    def scatter(group):
        to_tp(lambda j: part_tx[group].at[j], part_rx[group].at[me], part_recv.at[group])
        to_tp(lambda j: sq_tx.at[group], sq_rx.at[group, me], sq_recv.at[group])
        sq_rx[group, me] = sq_tx[group]
        part_rx[group][me] = part_tx[group][me]

    def hidden_of(squares, parts, n):
        total = jnp.zeros((1, 128), F32)
        gate = jnp.zeros((n, chunk), F32)
        up = jnp.zeros((n, chunk), F32)
        for j in range(ntp):
            total = total + squares[j]
            gate = gate + parts[j, 0].astype(F32)
            up = up + parts[j, 1].astype(F32)
        inv = lax.rsqrt(total / total_width + 1e-06) * UP_SCALE
        inv = col_of(inv, n, my_half * n)
        return (silu(gate * inv) * (up * inv)).astype(BF16)

    def tp_wait(buf, recv):
        some = buf.at[pl.ds(0, ntp - 1)]
        waiting(some, some, tp_send, recv).wait_recv()

    columns = pl.ds(pl.multiple_of(my_chunk * chunk, chunk), chunk)

    def reduce_group(group):
        half = 2 * (ends[group + 1] - ends[group])
        base = 4 * ends[group]
        with jax.named_scope(f"w_rs{group}"):
            tp_wait(part_rx[group], part_recv.at[group])
            tp_wait(sq_rx.at[group], sq_recv.at[group])
        hid_tx[group][...] = hidden_of(sq_rx.at[group], part_rx[group], half)
        own = hid.at[pl.ds(pl.multiple_of(base + my_half * half, half), half), columns]
        to_tp(lambda j: hid_tx[group], own, hid_recv.at[group])
        own[...] = hid_tx[group][...]

    shared_blocks = part_rx[groups - 1].at[pl.ds(0, ntp - 1), 0, pl.ds(0, 8)]

    def reduce_shared():
        with jax.named_scope("w_rss"):
            tp_wait(sq_rx.at[groups], sq_recv.at[groups])
            tp_wait(spart_rx, part_recv.at[groups])
        shid_tx[...] = hidden_of(sq_rx.at[groups], spart_rx, 8)
        own = shid.at[my_half, :, columns]
        to_tp(lambda j: shid_tx, own, hid_recv.at[groups])
        own[...] = shid_tx[...]

    def down_shared():
        with jax.named_scope("w_ags"):
            waiting(shared_blocks, shared_blocks, tp_send, hid_recv.at[groups]).wait_recv()
        hidden = jnp.concatenate([shid[0], shid[1]], axis=0)
        shared_out[...] = jnp.dot(hidden, sd[...], preferred_element_type=F32)

    def give_back(source):
        place_there = 2 * lax.rem(z - source - least + nz, nz) + c
        for core in range(2):

            @pl.when(2 * source + core != 2 * z + c)
            def _():
                pltpu.make_async_remote_copy(
                    src_ref=ret.at[2 * source + core],
                    dst_ref=back.at[place_there],
                    send_sem=ret_send,
                    recv_sem=ret_recv,
                    device_id=(source, core, y, x),
                    device_id_type=MESH,
                ).start()

    def down(group):
        low, high = ends[group], ends[group + 1]
        base, rows = 4 * low, 4 * (high - low)
        blocks = part_rx[group].at[pl.ds(0, ntp - 1), 0]
        with jax.named_scope(f"w_ag{group}"):
            waiting(blocks, blocks, tp_send, hid_recv.at[group]).wait_recv()
        result = jnp.dot(hid[base : base + rows, :], ed[...], preferred_element_type=F32)
        result = result.astype(BF16)
        for i in range(rows // 2):
            ret[2 * low + i] = result[2 * i : 2 * i + 2, :]

        def one(i, carry):
            give_back(low + i)
            return carry

        lax.fori_loop(0, high - low, one, 0)

    for i in (6, 7, 8, 9):
        loads[i].wait()
    reduce_shared()
    gate_up(0)
    scatter(0)
    gate_up(1)
    scatter(1)
    gate_up(2)
    scatter(2)
    down_shared()
    reduce_group(0)
    reduce_group(1)
    down(0)
    reduce_group(2)
    down(1)
    down(2)
    back[c - 2 * least] = ret[2 * z + c]

    got = back.at[pl.ds(0, 2 * nz - 1)]
    with jax.named_scope("w_back"):
        waiting(got, got, ret_send, ret_recv).wait_recv()
    terms = jnp.dot(
        slotw[...], back[...].reshape(slots, width), preferred_element_type=F32
    )
    routed = terms[0:16, :] + (terms[16:32, :] + terms[32:48, :])
    out_ref[...] = (shared_out[...] + routed)[0:tok_n, :].astype(BF16)

    def left(ref, sem):
        waiting(ref, ref, sem, ret_recv).wait_send()

    left(got, ret_send)
    left(msg.at[pl.ds(0, 2 * (n_plus + n_minus))], disp_send)
    left(msg.at[pl.ds(0, 4 * hop + 1)], disp_send)

    @pl.when(c == 1)
    def _():
        left(relay_p, rel_send)
        left(relay_m, rel_send)

    left(spart_rx.at[pl.ds(0, ntp - 1)], tp_send)
    left(shared_blocks, tp_send)
    for group in range(groups):
        left(part_rx[group].at[pl.ds(0, ntp - 1)], tp_send)
        left(part_rx[group].at[pl.ds(0, ntp - 1), 0], tp_send)
    for group in range(groups + 1):
        left(sq_rx.at[group, pl.ds(0, ntp - 1)], tp_send)


def local(sizes, tokens, norm_gain, routes, route_weights, eg, eu, ed, sg, su, sd):
    nz, ny, nx, hop = sizes
    ntp = ny * nx
    tok_n, width = tokens.shape
    picks = routes.shape[1]
    ff = eg.shape[2]
    chunk = ff // (ntp // 2)
    slots = 4 * nz
    ends = rings(nz)
    groups = len(ends) - 1
    halves = [2 * (high - low) for low, high in zip(ends, ends[1:])]
    n_plus, n_minus = nz // 2 - hop, nz // 2 - 1 - hop
    vm, dma = pltpu.VMEM, pltpu.SemaphoreType.DMA
    scratch = [
        vm((tok_n, width), BF16),
        vm((1, width), F32),
        vm((picks, tok_n), jnp.int32),
        vm((picks, tok_n), F32),
        vm((width, ff), BF16),
        vm((width, ff), BF16),
        vm((ff, width), BF16),
        vm((width, ff), BF16),
        vm((width, ff), BF16),
        vm((ff, width), BF16),
        vm((16, width), BF16),
        vm((picks, 16), jnp.int32),
        vm((picks, 16), F32),
        vm((48, slots), BF16),
        vm((16, width), F32),
        vm((slots // 2, 2, width), BF16),
        vm((2 * n_plus, 2, 2, width), BF16),
        vm((2 * n_minus, 2, 2, width), BF16),
        vm((slots // 2, 2, width), BF16),
        vm((groups + 1, 1, 128), F32),
        vm((groups + 1, ntp, 1, 128), F32),
        vm((ntp, 2, 8, chunk), F32),
        vm((ntp, 2, 8, chunk), F32),
        vm((8, chunk), BF16),
        vm((2, 8, ff), BF16),
        vm((slots, ff), BF16),
        vm((slots // 2, 2, width), BF16),
        vm((slots // 2, 2, width), BF16),
        [vm((ntp, 2, half, chunk), BF16) for half in halves],
        [vm((ntp, 2, half, chunk), BF16) for half in halves],
        [vm((half, chunk), BF16) for half in halves],
        dma((10,)),
        dma,
        dma((groups,)),
        dma,
        dma((2,)),
        dma,
        dma((groups + 1,)),
        dma((groups + 1,)),
        dma((groups + 1,)),
        dma,
        dma,
        pltpu.SemaphoreType.REGULAR((4,)),
    ]
    return pl.pallas_call(
        functools.partial(kernel, sizes),
        out_shape=jax.ShapeDtypeStruct((tok_n, width), BF16),
        in_specs=[pl.BlockSpec(memory_space=pl.ANY)] * 10,
        out_specs=pl.BlockSpec(memory_space=pltpu.VMEM),
        scratch_shapes=scratch,
        compiler_params=pltpu.CompilerParams(collective_id=0, has_side_effects=True),
        name="moe_step",
    )(tokens, norm_gain.reshape(1, width), routes.T, route_weights.T, eg, eu, ed, sg, su, sd)


def on_torus(torus):
    n = torus.shape
    sizes = (n["z"], n["y"], n["x"], (3 * n["z"] + 14) // 16)
    ep, tp = ("z", "c"), ("y", "x")
    in_specs = (
        P(ep, tp),
        P(tp),
        P(ep, None),
        P(ep, None),
        P(ep, tp, None),
        P(ep, tp, None),
        P(ep, None, tp),
        P(tp, None),
        P(tp, None),
        P(None, tp),
    )
    return jax.shard_map(
        functools.partial(local, sizes),
        mesh=torus,
        in_specs=in_specs,
        out_specs=P(ep, tp),
        check_vma=False,
    )


def solution(mesh):
    return on_torus(Mesh(mesh.devices.reshape(32, 2, 4, 4), ("z", "c", "y", "x")))
```

time: 69.4 us -> 64.5 us (0.929)
  Pallas kernels: 65.7 us -> 62.9 us
  local copies, waits for them, and re-layouts: 3.35 us -> 1.3 us
    pallas_call x1, Pallas kernels: 65.7 us -> 62.9 us  [local(): pl.pallas_call(functools.partial(kernel, sizes), out_shape=jax.ShapeDtype...]
    unnamed x5 -> x1, local copies, waits for them, and re-layouts: 3.35 us -> 1.3 us
where the time goes in v2:
time: 64.5 us; the launch traced here: 64.2 us
  Pallas kernels  62.9 us (98%)
  local copies, waits for them, and re-layouts  1.3 us (2%)
    pallas_call x1, Pallas kernels, local(): pl.pallas_call(functools.partial(kernel, sizes), out_shape=jax.ShapeDtype...  62.9 us
    unnamed x1, local copies, waits for them, and re-layouts  1.3 us

profile of v2, /device:TPU:1, one launch (start us, length us, event | category | flops | bytes accessed | tf_op | source)
XLA Modules:
  0.0 64.2 jit_solution(12624367342276210345)
XLA Ops:
  0.0 62.9 %moe_step.1 = bf16[12,256]{1,0:T(8,128)(2,1)} custom-call(bf16[12,256]{1,0:T(8,128)(2,1)} %tok_hbm.1, f32[1,256]{1,0:T(1,128)} %bitcast.5, s32[6,12]{1,0:T(8,128)} %bitcast.3, f32[6,12]{1,0:T(8,128)} %bitcast.4, bf16[1,256,1024]{2,1,0:T(8,128)(2,1)} %eg_hbm.1, bf16[1,256,1024]{2,1,0:T(8,128)(2,1)} %eu_hbm.1, bf16[1,1024,256]{2,1,0:T(8,128)(2,1)} %ed_hbm.1, ...), custom_call_target="tpu_custom_call" | custom-call | tf_op jit(solution)/shard_map/moe_step/pallas_call | solution.py:549
  62.9 1.3 %copy.12 = bf16[12,256]{1,0:T(8,128)(2,1)} copy(bf16[12,256]{1,0:T(8,128)(2,1)} %moe_step.1) | data formatting | bytes 12288

commit v3 on v2

--- a/solution.py
+++ b/solution.py
@@ -25,6 +25,13 @@
         jnp.int32, (rows, width), 1
     )
     return jnp.sum(jnp.where(eye, col, 0.0), axis=0, keepdims=True)
+
+
+def three_terms(v):
+    high = v.astype(BF16)
+    rest = v - high.astype(F32)
+    middle = rest.astype(BF16)
+    return high, middle, (rest - middle.astype(F32)).astype(BF16)
 
 
 def col_of(row, rows, first):
@@ -71,8 +78,6 @@
     relay_p,
     relay_m,
     rx,
-    sq_tx,
-    sq_rx,
     spart_tx,
     spart_rx,
     shid_tx,
@@ -89,7 +94,6 @@
     rel_send,
     rel_recv,
     tp_send,
-    sq_recv,
     part_recv,
     hid_recv,
     ret_send,
@@ -121,7 +125,7 @@
 
     def peer(i):
         j = lax.rem(me + i, ntp)
-        return j, (z, c, j // nx, lax.rem(j, nx))
+        return j, (z, c, lax.div(j, nx), lax.rem(j, nx))
 
     barrier = pltpu.get_barrier_semaphore()
 
@@ -133,13 +137,18 @@
                 )
         return carry
 
-    def greet_tp(i, carry):
-        pl.semaphore_signal(barrier, inc=1, device_id=peer(i)[1], device_id_type=MESH)
-        return carry
+    def in_row(i):
+        return z, c, y, lax.rem(x + i, nx)
+
+    def in_column(i):
+        return z, c, lax.rem(y + i, ny), x
 
     lax.fori_loop(0, close, greet_z, 0)
     pl.semaphore_signal(barrier, inc=1, device_id=(z, 1 - c, y, x), device_id_type=MESH)
-    lax.fori_loop(1, ntp, greet_tp, 0)
+    for i in range(1, nx):
+        pl.semaphore_signal(barrier, inc=1, device_id=in_row(i), device_id_type=MESH)
+    for i in range(1, ny):
+        pl.semaphore_signal(barrier, inc=1, device_id=in_column(i), device_id_type=MESH)
 
     loads = []
     for i, (src, dst) in enumerate(
@@ -194,7 +203,7 @@
         msg[i] = outgoing[2 * i : 2 * i + 2, :]
 
     with jax.named_scope("w_barrier"):
-        pl.semaphore_wait(barrier, 4 * close + 1 + ntp - 1)
+        pl.semaphore_wait(barrier, 4 * close + 1 + nx - 1 + ny - 1)
 
     def tell(sem, d, core):
         pl.semaphore_signal(sem, inc=1, device_id=(at(d), core, y, x), device_id_type=MESH)
@@ -238,16 +247,18 @@
     with jax.named_scope("w_plus"):
         pl.semaphore_wait(entered.at[0], 1)
     bundle(hop + 1, n_plus, relay_p, at(hop), 0).start()
-    lax.fori_loop(0, hop, near_plus, 0)
     with jax.named_scope("w_minus"):
         pl.semaphore_wait(entered.at[1], 1)
-    bundle(least, n_minus, relay_m, at(-hop), 1).start()
 
     @pl.when(c == 1)
     def _():
         tell(entered.at[2], -hop, 1)
         tell(entered.at[3], hop, 1)
 
+    bundle(least, n_minus, relay_m, at(-hop), 1).start()
+    for i in range(1, ny):
+        pl.semaphore_signal(entered.at[4], inc=1, device_id=in_column(i), device_id_type=MESH)
+    lax.fori_loop(0, hop, near_plus, 0)
     lax.fori_loop(0, hop, near_minus, 0)
     send_near(0, 1 - c)
     rx[2 * z + c] = msg[c - 2 * least]
@@ -280,18 +291,22 @@
     gains = gain[...] * DOWN_SCALE
     values = tokens16.astype(F32)
     scaled_tok = (values * gains).astype(BF16)
-    sq_tx[groups] = row_of(jnp.sum(values * values, axis=1, keepdims=True), 128)
-    sq_rx[groups, me] = sq_tx[groups]
+    squares = row_of(jnp.sum(values * values, axis=1, keepdims=True), 128)
+    for j in range(ntp):
+        spart_tx[j, 16:24] = jnp.concatenate([squares, jnp.zeros((7, 128), F32)], axis=0)
     for i in (4, 5):
         loads[i].wait()
     for n, w in enumerate((sg, su)):
         part = jnp.dot(scaled_tok, w[...], preferred_element_type=F32)
         for k in range(ntp // 2):
             for h in range(2):
-                spart_tx[2 * k + h, n] = part[8 * h : 8 * h + 8, k * chunk : (k + 1) * chunk]
+                spart_tx[2 * k + h, 8 * n : 8 * n + 8] = part[
+                    8 * h : 8 * h + 8, k * chunk : (k + 1) * chunk
+                ]
     spart_rx[me] = spart_tx[me]
 
-    to_tp(lambda j: sq_tx.at[groups], sq_rx.at[groups, me], sq_recv.at[groups])
+    if ny > 1:
+        pl.semaphore_wait(entered.at[4], ny - 1)
     slot_weight = slot_weight.T
     for i in range(3):
         term = slot_weight.astype(BF16)
@@ -310,27 +325,39 @@
                 device_id_type=MESH,
             ).start()
 
-    @pl.when(c == 1)
-    def _():
+    def relay_up():
         with jax.named_scope("w_entered"):
             pl.semaphore_wait(entered.at[2], 1)
         with jax.named_scope("w_relp"):
             waiting(relay_p, relay_p, rel_send, rel_recv.at[0]).wait_recv()
 
-        def forward_plus(k, carry):
+        def one(k, carry):
             forward(relay_p, n_plus - 1 - k, at(-hop), 1)
             return carry
 
-        lax.fori_loop(0, n_plus, forward_plus, 0)
-        pl.semaphore_wait(entered.at[3], 1)
+        lax.fori_loop(0, n_plus, one, 0)
+
+    def relay_down():
+        with jax.named_scope("w_entered"):
+            pl.semaphore_wait(entered.at[3], 1)
         with jax.named_scope("w_relm"):
             waiting(relay_m, relay_m, rel_send, rel_recv.at[1]).wait_recv()
 
-        def forward_minus(i, carry):
+        def one(i, carry):
             forward(relay_m, i, at(hop), hop + least)
             return carry
 
-        lax.fori_loop(0, n_minus, forward_minus, 0)
+        lax.fori_loop(0, n_minus, one, 0)
+
+    @pl.when(jnp.logical_and(c == 1, z < nz - hop))
+    def _():
+        relay_up()
+        relay_down()
+
+    @pl.when(jnp.logical_and(c == 1, z >= nz - hop))
+    def _():
+        relay_down()
+        relay_up()
 
     def gate_up(group):
         first, last = 2 * ends[group], 2 * ends[group + 1]
@@ -351,25 +378,27 @@
             part = jnp.dot(lhs, w[...], preferred_element_type=F32).astype(BF16)
             for k in range(ntp // 2):
                 for h in range(2):
-                    part_tx[group][2 * k + h, n] = part[
+                    part_tx[group][2 * k + h, half * n : half * (n + 1)] = part[
                         half * h : half * (h + 1), k * chunk : (k + 1) * chunk
                     ]
-        sq_tx[group] = row_of(jnp.sum(values * values, axis=1, keepdims=True), 128)
+        squares = row_of(jnp.sum(values * values, axis=1, keepdims=True), 128)
+        terms = jnp.concatenate([*three_terms(squares), jnp.zeros((5, 128), BF16)], axis=0)
+        for j in range(ntp):
+            part_tx[group][j, 2 * half : 2 * half + 8] = terms
 
     def scatter(group):
         to_tp(lambda j: part_tx[group].at[j], part_rx[group].at[me], part_recv.at[group])
-        to_tp(lambda j: sq_tx.at[group], sq_rx.at[group, me], sq_recv.at[group])
-        sq_rx[group, me] = sq_tx[group]
         part_rx[group][me] = part_tx[group][me]
 
-    def hidden_of(squares, parts, n):
-        total = jnp.zeros((1, 128), F32)
+    def hidden_of(parts, n):
         gate = jnp.zeros((n, chunk), F32)
         up = jnp.zeros((n, chunk), F32)
+        total = jnp.zeros((8, 128), F32)
         for j in range(ntp):
-            total = total + squares[j]
-            gate = gate + parts[j, 0].astype(F32)
-            up = up + parts[j, 1].astype(F32)
+            gate = gate + parts[j, 0:n].astype(F32)
+            up = up + parts[j, n : 2 * n].astype(F32)
+            total = total + parts[j, 2 * n : 2 * n + 8].astype(F32)
+        total = total[0:1] + (total[1:2] + total[2:3])
         inv = lax.rsqrt(total / total_width + 1e-06) * UP_SCALE
         inv = col_of(inv, n, my_half * n)
         return (silu(gate * inv) * (up * inv)).astype(BF16)
@@ -385,19 +414,17 @@
         base = 4 * ends[group]
         with jax.named_scope(f"w_rs{group}"):
             tp_wait(part_rx[group], part_recv.at[group])
-            tp_wait(sq_rx.at[group], sq_recv.at[group])
-        hid_tx[group][...] = hidden_of(sq_rx.at[group], part_rx[group], half)
+        hid_tx[group][...] = hidden_of(part_rx[group], half)
         own = hid.at[pl.ds(pl.multiple_of(base + my_half * half, half), half), columns]
         to_tp(lambda j: hid_tx[group], own, hid_recv.at[group])
         own[...] = hid_tx[group][...]
 
-    shared_blocks = part_rx[groups - 1].at[pl.ds(0, ntp - 1), 0, pl.ds(0, 8)]
+    shared_blocks = part_rx[groups - 1].at[pl.ds(0, ntp - 1), pl.ds(0, 8)]
 
     def reduce_shared():
         with jax.named_scope("w_rss"):
-            tp_wait(sq_rx.at[groups], sq_recv.at[groups])
             tp_wait(spart_rx, part_recv.at[groups])
-        shid_tx[...] = hidden_of(sq_rx.at[groups], spart_rx, 8)
+        shid_tx[...] = hidden_of(spart_rx, 8)
         own = shid.at[my_half, :, columns]
         to_tp(lambda j: shid_tx, own, hid_recv.at[groups])
         own[...] = shid_tx[...]
@@ -426,7 +453,7 @@
     def down(group):
         low, high = ends[group], ends[group + 1]
         base, rows = 4 * low, 4 * (high - low)
-        blocks = part_rx[group].at[pl.ds(0, ntp - 1), 0]
+        blocks = part_rx[group].at[pl.ds(0, ntp - 1), pl.ds(0, rows // 2)]
         with jax.named_scope(f"w_ag{group}"):
             waiting(blocks, blocks, tp_send, hid_recv.at[group]).wait_recv()
         result = jnp.dot(hid[base : base + rows, :], ed[...], preferred_element_type=F32)
@@ -446,15 +473,15 @@
     gate_up(0)
     scatter(0)
     gate_up(1)
-    scatter(1)
     gate_up(2)
-    scatter(2)
     down_shared()
     reduce_group(0)
+    scatter(1)
+    down(0)
+    scatter(2)
     reduce_group(1)
-    down(0)
+    down(1)
     reduce_group(2)
-    down(1)
     down(2)
     back[c - 2 * least] = ret[2 * z + c]
 
@@ -483,9 +510,8 @@
     left(shared_blocks, tp_send)
     for group in range(groups):
         left(part_rx[group].at[pl.ds(0, ntp - 1)], tp_send)
-        left(part_rx[group].at[pl.ds(0, ntp - 1), 0], tp_send)
-    for group in range(groups + 1):
-        left(sq_rx.at[group, pl.ds(0, ntp - 1)], tp_send)
+        half = 2 * (ends[group + 1] - ends[group])
+        left(part_rx[group].at[pl.ds(0, ntp - 1), pl.ds(0, half)], tp_send)
 
 
 def local(sizes, tokens, norm_gain, routes, route_weights, eg, eu, ed, sg, su, sd):
@@ -521,17 +547,15 @@
         vm((2 * n_plus, 2, 2, width), BF16),
         vm((2 * n_minus, 2, 2, width), BF16),
         vm((slots // 2, 2, width), BF16),
-        vm((groups + 1, 1, 128), F32),
-        vm((groups + 1, ntp, 1, 128), F32),
-        vm((ntp, 2, 8, chunk), F32),
-        vm((ntp, 2, 8, chunk), F32),
+        vm((ntp, 24, chunk), F32),
+        vm((ntp, 24, chunk), F32),
         vm((8, chunk), BF16),
         vm((2, 8, ff), BF16),
         vm((slots, ff), BF16),
         vm((slots // 2, 2, width), BF16),
         vm((slots // 2, 2, width), BF16),
-        [vm((ntp, 2, half, chunk), BF16) for half in halves],
-        [vm((ntp, 2, half, chunk), BF16) for half in halves],
+        [vm((ntp, 2 * half + 8, chunk), BF16) for half in halves],
+        [vm((ntp, 2 * half + 8, chunk), BF16) for half in halves],
         [vm((half, chunk), BF16) for half in halves],
         dma((10,)),
         dma,
@@ -541,10 +565,9 @@
         dma,
         dma((groups + 1,)),
         dma((groups + 1,)),
-        dma((groups + 1,)),
         dma,
         dma,
-        pltpu.SemaphoreType.REGULAR((4,)),
+        pltpu.SemaphoreType.REGULAR((5,)),
     ]
     return pl.pallas_call(
         functools.partial(kernel, sizes),

time: 64.5 us -> 62.4 us (0.967)
  Pallas kernels: 62.9 us -> 60.7 us
    pallas_call x1, Pallas kernels: 62.9 us -> 60.7 us  [local(): pl.pallas_call(functools.partial(kernel, sizes), out_shape=jax.ShapeDtype...]
where the time goes in v3:
time: 62.4 us; the launch traced here: 62 us
  Pallas kernels  60.7 us (97%)
  local copies, waits for them, and re-layouts  1.3 us (2%)
    pallas_call x1, Pallas kernels, local(): pl.pallas_call(functools.partial(kernel, sizes), out_shape=jax.ShapeDtype...  60.7 us
    unnamed x1, local copies, waits for them, and re-layouts  1.3 us

profile of v3, /device:TPU:1, one launch (start us, length us, event | category | flops | bytes accessed | tf_op | source)
XLA Modules:
  0.0 62.0 jit_solution(10340904940534905857)
XLA Ops:
  0.0 60.7 %moe_step.1 = bf16[12,256]{1,0:T(8,128)(2,1)} custom-call(bf16[12,256]{1,0:T(8,128)(2,1)} %tok_hbm.1, f32[1,256]{1,0:T(1,128)} %bitcast.5, s32[6,12]{1,0:T(8,128)} %bitcast.3, f32[6,12]{1,0:T(8,128)} %bitcast.4, bf16[1,256,1024]{2,1,0:T(8,128)(2,1)} %eg_hbm.1, bf16[1,256,1024]{2,1,0:T(8,128)(2,1)} %eu_hbm.1, bf16[1,1024,256]{2,1,0:T(8,128)(2,1)} %ed_hbm.1, ...), custom_call_target="tpu_custom_call" | custom-call | tf_op jit(solution)/shard_map/moe_step/pallas_call | solution.py:572
  60.7 1.3 %copy.12 = bf16[12,256]{1,0:T(8,128)(2,1)} copy(bf16[12,256]{1,0:T(8,128)(2,1)} %moe_step.1) | data formatting | bytes 12288

commit v4 on v3

--- a/solution.py
+++ b/solution.py
@@ -569,15 +569,18 @@
         dma,
         pltpu.SemaphoreType.REGULAR((5,)),
     ]
+    def held(a):
+        return pltpu.with_memory_space_constraint(a, pltpu.HBM)
+
     return pl.pallas_call(
         functools.partial(kernel, sizes),
         out_shape=jax.ShapeDtypeStruct((tok_n, width), BF16),
         in_specs=[pl.BlockSpec(memory_space=pl.ANY)] * 10,
         out_specs=pl.BlockSpec(memory_space=pltpu.VMEM),
         scratch_shapes=scratch,
-        compiler_params=pltpu.CompilerParams(collective_id=0, has_side_effects=True),
+        compiler_params=pltpu.CompilerParams(collective_id=0, has_side_effects=True, vmem_limit_bytes=40 << 20),
         name="moe_step",
-    )(tokens, norm_gain.reshape(1, width), routes.T, route_weights.T, eg, eu, ed, sg, su, sd)
+    )(*map(held, (tokens, norm_gain.reshape(1, width), routes.T, route_weights.T, eg, eu, ed, sg, su, sd)))
 
 
 def on_torus(torus):

time: 62.4 us -> 61 us (0.978)
  local copies, waits for them, and re-layouts: 1.3 us -> 0.6 us
    unnamed x1, local copies, waits for them, and re-layouts: 1.3 us -> 0.6 us
where the time goes in v4:
time: 61 us; the launch traced here: 60.7 us
  Pallas kernels  60.1 us (99%)
    pallas_call x1, Pallas kernels, local(): pl.pallas_call(functools.partial(kernel, sizes), out_shape=jax.ShapeDtype...  60.1 us

profile of v4, /device:TPU:1, one launch (start us, length us, event | category | flops | bytes accessed | tf_op | source)
XLA Modules:
  0.0 60.7 jit_solution(13503602385343825190)
XLA Ops:
  0.0 60.1 %moe_step.1 = bf16[12,256]{1,0:T(8,128)(2,1)S(1)} custom-call(bf16[12,256]{1,0:T(8,128)(2,1)} %tok_hbm.1, f32[1,256]{1,0:T(1,128)} %bitcast.5, s32[6,12]{1,0:T(8,128)} %bitcast.3, f32[6,12]{1,0:T(8,128)} %bitcast.4, bf16[1,256,1024]{2,1,0:T(8,128)(2,1)} %eg_hbm.1, bf16[1,256,1024]{2,1,0:T(8,128)(2,1)} %eu_hbm.1, bf16[1,1024,256]{2,1,0:T(8,128)(2,1)} %ed_hbm.1, ...), custom_call_target="tpu_custom_call" | custom-call | tf_op jit(solution)/shard_map/moe_step/pallas_call | solution.py:575
  60.1 0.6 copy.12

commit v5 on v4

--- a/solution.py
+++ b/solution.py
@@ -43,7 +43,7 @@
 
 
 def rings(nz):
-    return (0, nz // 4, nz // 2, nz)
+    return (0, nz // 8, 3 * nz // 8, nz)
 
 
 def kernel(
@@ -222,7 +222,8 @@
         )
 
     def ring(source):
-        return source // ends[1] - source // (3 * ends[1])
+        place, step = source + ends[1], 2 * ends[1]
+        return place // step - place // (3 * step) - place // (4 * step)
 
     def send_near(d, core):
         pltpu.make_async_remote_copy(
@@ -411,11 +412,10 @@
 
     def reduce_group(group):
         half = 2 * (ends[group + 1] - ends[group])
-        base = 4 * ends[group]
         with jax.named_scope(f"w_rs{group}"):
             tp_wait(part_rx[group], part_recv.at[group])
         hid_tx[group][...] = hidden_of(part_rx[group], half)
-        own = hid.at[pl.ds(pl.multiple_of(base + my_half * half, half), half), columns]
+        own = hid[group].at[my_half, :, columns]
         to_tp(lambda j: hid_tx[group], own, hid_recv.at[group])
         own[...] = hid_tx[group][...]
 
@@ -452,11 +452,12 @@
 
     def down(group):
         low, high = ends[group], ends[group + 1]
-        base, rows = 4 * low, 4 * (high - low)
+        rows = 4 * (high - low)
         blocks = part_rx[group].at[pl.ds(0, ntp - 1), pl.ds(0, rows // 2)]
         with jax.named_scope(f"w_ag{group}"):
             waiting(blocks, blocks, tp_send, hid_recv.at[group]).wait_recv()
-        result = jnp.dot(hid[base : base + rows, :], ed[...], preferred_element_type=F32)
+        hidden = jnp.concatenate([hid[group][0], hid[group][1]], axis=0)
+        result = jnp.dot(hidden, ed[...], preferred_element_type=F32)
         result = result.astype(BF16)
         for i in range(rows // 2):
             ret[2 * low + i] = result[2 * i : 2 * i + 2, :]
@@ -473,13 +474,13 @@
     gate_up(0)
     scatter(0)
     gate_up(1)
+    scatter(1)
     gate_up(2)
     down_shared()
     reduce_group(0)
-    scatter(1)
+    reduce_group(1)
     down(0)
     scatter(2)
-    reduce_group(1)
     down(1)
     reduce_group(2)
     down(2)
@@ -551,7 +552,7 @@
         vm((ntp, 24, chunk), F32),
         vm((8, chunk), BF16),
         vm((2, 8, ff), BF16),
-        vm((slots, ff), BF16),
+        [vm((2, half, ff), BF16) for half in halves],
         vm((slots // 2, 2, width), BF16),
         vm((slots // 2, 2, width), BF16),
         [vm((ntp, 2 * half + 8, chunk), BF16) for half in halves],

time: 61 us -> 60.6 us (level)
  no operation moved by 1% of the time
where the time goes in v5:
time: 60.6 us; the launch traced here: 60.4 us
  Pallas kernels  59.8 us (99%)
    pallas_call x1, Pallas kernels, local(): pl.pallas_call(functools.partial(kernel, sizes), out_shape=jax.ShapeDtype...  59.8 us

profile of v5, /device:TPU:1, one launch (start us, length us, event | category | flops | bytes accessed | tf_op | source)
XLA Modules:
  0.0 60.4 jit_solution(11792864510943861215)
XLA Ops:
  0.0 59.8 %moe_step.1 = bf16[12,256]{1,0:T(8,128)(2,1)S(1)} custom-call(bf16[12,256]{1,0:T(8,128)(2,1)} %tok_hbm.1, f32[1,256]{1,0:T(1,128)} %bitcast.5, s32[6,12]{1,0:T(8,128)} %bitcast.3, f32[6,12]{1,0:T(8,128)} %bitcast.4, bf16[1,256,1024]{2,1,0:T(8,128)(2,1)} %eg_hbm.1, bf16[1,256,1024]{2,1,0:T(8,128)(2,1)} %eu_hbm.1, bf16[1,1024,256]{2,1,0:T(8,128)(2,1)} %ed_hbm.1, ...), custom_call_target="tpu_custom_call" | custom-call | tf_op jit(solution)/shard_map/moe_step/pallas_call | solution.py:576
  59.8 0.6 copy.12
